TPU v7x, 32 devices: a whole 2x2x4 slice. The times are simulated.
32 devices in a mesh: ep: 8 (over z, x), tp: 4 (over y, core).
Axes of the slice: x: 2, y: 2, z: 4, core: 2. Of those that a mesh axis runs over, the one named last changes fastest.
Arguments:
- queries: bfloat16 [4096, 2048], P('ep', 'tp'), may hold values from -5 to 5
- key_rows: bfloat16 [4096, 2048], P('ep', 'tp'), may hold values from -5 to 5
- values: bfloat16 [4096, 2048], P('ep', 'tp'), may hold values from -6 to 6
- forget_log: float32 [4096, 16], P(None, 'tp'), may hold values from -515 to 0, as said below
- out_weight: bfloat16 [2048, 4096], P(None, 'tp'), may hold values from -1 to 1
- expert_input: bfloat16 [1024, 4096], P(('ep', 'tp')), may hold values from -6 to 6
- norm_gain: float32 [4096], replicated, may hold values from 0.1 to 1.9
- route_ids: int32 [1024, 2], P('ep'), may hold values from 0 to 7, all different within a row; in each aligned block of 128 rows (0 to 127, 128 to 255, ...) at most 64 rows name the same one
- route_weights: float32 [1024, 2], P('ep'), may hold values from 0.2 to 1
- gate_weight: bfloat16 [8, 4096, 2048], P('ep', None, 'tp'), may hold values from -0.09375 to 0.09375
- up_weight: bfloat16 [8, 4096, 2048], P('ep', None, 'tp'), may hold values from -0.09375 to 0.09375
- down_weight: bfloat16 [8, 2048, 4096], P('ep', None, 'tp'), may hold values from -0.125 to 0.125
Outputs:
- mixer_out: bfloat16 [4096, 4096], P('ep', 'tp')
- expert_out: bfloat16 [1024, 4096], P('ep', 'tp')
Inputs may be any that keep to these rules, and one draw needn't show every extreme that they name: forget_log[t, h] is the sum of the log forget gates of head h at positions 0 to t of the one sequence; it never rises along positions. `route_ids`: each row names 2 different experts. In each aligned block of 128 rows (the rows of one index of ep) no expert is named by more than 64 rows, and some block reaches 64.
All inputs are finite; a program needn't handle non-finite values.
Results may differ from a plain program's by a relative error of at most 0.0071.
Values may be sent and summed in bfloat16 or wider, within the bound.
A program may use at most 64 MiB of HBM per device.

v0:
```python
import jax
import jax.numpy as jnp
from jax import lax
from jax.sharding import PartitionSpec as P

EPSILON = 1e-05


def slot_places(route_rows, experts, capacity):
    entries = route_rows.reshape(-1)
    matches = (entries[:, None] == jnp.arange(experts, dtype=jnp.int32)[None, :]).astype(jnp.int32)
    earlier = jnp.cumsum(matches, axis=0) - matches
    ranking = jnp.sum(earlier * matches, axis=1)
    return entries * capacity + ranking


def source_table(places, rows_count, chosen, total_slots):
    owners = jnp.arange(places.shape[0], dtype=jnp.int32) // chosen
    return jnp.full((total_slots,), rows_count, jnp.int32).at[places].set(owners)


def body(
    queries,
    key_rows,
    values,
    forget_log,
    out_weight,
    expert_input,
    norm_gain,
    route_ids,
    route_weights,
    gate_weight,
    up_weight,
    down_weight,
):
    row_count = queries.shape[0]
    heads_here = forget_log.shape[1]
    head_width = queries.shape[1] // heads_here
    own_start = lax.axis_index("ep") * row_count
    position_indices = own_start + jnp.arange(row_count, dtype=jnp.int32)
    query_heads = queries.reshape(row_count, heads_here, head_width)
    query_gate = lax.dynamic_slice_in_dim(forget_log, own_start, row_count, 0)
    score_scale = head_width ** (-0.5)

    def fold_shard(state_now, shard_item):
        first_row, key_shard, value_shard = shard_item

        def attend(state_in):
            row_max, row_total, weighted = state_in
            key_heads = key_shard.reshape(row_count, heads_here, head_width)
            value_heads = value_shard.reshape(row_count, heads_here, head_width)
            key_gate = lax.dynamic_slice_in_dim(forget_log, first_row, row_count, 0)
            scores = (
                jnp.einsum(
                    "qhd,khd->hqk", query_heads, key_heads, preferred_element_type=jnp.float32
                )
                * score_scale
            )
            scores = scores + query_gate.T[:, :, None] - key_gate.T[:, None, :]
            key_pos = first_row + jnp.arange(row_count, dtype=jnp.int32)
            scores = jnp.where(
                key_pos[None, None, :] <= position_indices[None, :, None], scores, -jnp.inf
            )
            newest = jnp.maximum(row_max, jnp.max(scores, axis=2))
            factor = jnp.exp(row_max - newest)
            weights_now = jnp.exp(scores - newest[:, :, None])
            row_total = row_total * factor + jnp.sum(weights_now, axis=2)
            weighted = weighted * factor[:, :, None] + jnp.einsum(
                "hqk,khd->hqd",
                weights_now.astype(jnp.bfloat16),
                value_heads,
                preferred_element_type=jnp.float32,
            )
            return (newest, row_total, weighted)

        return (
            lax.cond(first_row <= own_start, attend, lambda state_in: state_in, state_now),
            None,
        )

    initial = (
        jnp.full((heads_here, row_count), -jnp.inf, jnp.float32),
        jnp.zeros((heads_here, row_count), jnp.float32),
        jnp.zeros((heads_here, row_count, head_width), jnp.float32),
    )
    state_now = initial
    key_piece = lax.all_gather(key_rows, "ep", axis=0, tiled=True)
    value_piece = lax.all_gather(values, "ep", axis=0, tiled=True)
    shards = key_piece.shape[0] // row_count
    starts = row_count * jnp.arange(shards, dtype=jnp.int32)
    stacked = (
        starts,
        key_piece.reshape(shards, row_count, -1),
        value_piece.reshape(shards, row_count, -1),
    )
    state_now, _ = lax.scan(fold_shard, state_now, stacked)
    row_max, row_total, weighted = state_now
    attended = (
        (weighted / row_total[:, :, None])
        .transpose(1, 0, 2)
        .reshape(row_count, heads_here * head_width)
        .astype(jnp.bfloat16)
    )
    as_float = expert_input.astype(jnp.float32)
    center = jnp.mean(as_float, axis=1, keepdims=True)
    variance = jnp.mean(jnp.square(as_float - center), axis=1, keepdims=True)
    normed = ((as_float - center) * lax.rsqrt(variance + EPSILON) * norm_gain).astype(jnp.bfloat16)
    group_rows = lax.all_gather(normed, "tp", axis=0, tiled=True)
    block_rows = route_ids.shape[0]
    chosen = route_ids.shape[1]
    expert_local = gate_weight.shape[0]
    ep_count = lax.axis_size("ep")
    tp_count = lax.axis_size("tp")
    experts = expert_local * ep_count
    capacity = block_rows * chosen * 2 // experts
    places = slot_places(route_ids, experts, capacity)
    slot_table = source_table(places, block_rows, chosen, experts * capacity).reshape(
        ep_count, expert_local, capacity
    )
    share_size = capacity // tp_count
    part_table = lax.dynamic_slice_in_dim(
        slot_table, lax.axis_index("tp") * share_size, share_size, 2
    )
    outgoing = jnp.take(group_rows, part_table, axis=0, mode="fill", fill_value=0)
    arrived = lax.all_to_all(outgoing, "ep", split_axis=0, concat_axis=0, tiled=True)
    arrived_rows = lax.all_gather(arrived, "tp", axis=2, tiled=True)
    gate_part = jnp.einsum(
        "sxcd,xdf->sxcf", arrived_rows, gate_weight, preferred_element_type=jnp.float32
    )
    up_part = jnp.einsum(
        "sxcd,xdf->sxcf", arrived_rows, up_weight, preferred_element_type=jnp.float32
    )
    hidden = (jax.nn.silu(gate_part) * up_part).astype(jnp.bfloat16)
    slots_all = ep_count * expert_local * capacity
    flat_hidden = hidden.reshape(slots_all, hidden.shape[3])
    out_width = out_weight.shape[1]
    mixer_sum = jnp.dot(
        lax.all_gather(attended, "tp", axis=1, tiled=True),
        out_weight,
        preferred_element_type=jnp.float32,
    )
    part_rows = lax.all_gather(flat_hidden, "tp", axis=1, tiled=True)
    shaped = part_rows.reshape(ep_count, expert_local, capacity, part_rows.shape[1])
    product = jnp.einsum("sxcf,xfd->sxcd", shaped, down_weight, preferred_element_type=jnp.float32)
    expert_sum = product.reshape(slots_all, out_width)
    leaving = expert_sum.astype(jnp.bfloat16).reshape(ep_count, expert_local, capacity, out_width)
    returned = lax.all_to_all(leaving, "ep", split_axis=0, concat_axis=0, tiled=True)
    picked = jnp.take(returned.reshape(experts * capacity, out_width), places, axis=0).astype(
        jnp.float32
    )
    combined = jnp.sum(
        (picked * route_weights.reshape(-1)[:, None]).reshape(block_rows, chosen, out_width), axis=1
    )
    return (mixer_sum.astype(jnp.bfloat16), combined.astype(jnp.bfloat16))


def solution(mesh):
    placed = (
        P("ep", "tp"),
        P("ep", "tp"),
        P("ep", "tp"),
        P(None, "tp"),
        P(None, "tp"),
        P(("ep", "tp"), None),
        P(),
        P("ep", None),
        P("ep", None),
        P("ep", None, "tp"),
        P("ep", None, "tp"),
        P("ep", None, "tp"),
    )
    return jax.shard_map(
        body, mesh=mesh, in_specs=placed, out_specs=(P("ep", "tp"), P("ep", "tp")), check_vma=False
    )
```

profile of v0, /device:TPU:0, one launch (start us, length us, event | category | flops | bytes accessed | tf_op | source)
XLA Modules:
  0.0 390.9 jit_solution(14663094674887229282)
XLA Ops:
  9.5 1.8 fusion.51
  14.4 1.4 scatter_custom_fusion
  16.0 14.9 %all-gather.13.cloned.1.call-done = bf16[128,4096]{1,0:T(8,128)(2,1)} async-done(((bf16[32,4096]{1,0:T(8,128)(2,1)}), bf16[128,4096]{1,0:T(8,128)(2,1)}) %all-gather.13.cloned.1.call-update) | async-done | bytes 1048592 | tf_op jit(solution)/shard_map/all_gather | solution.py:108
  30.9 3.6 gather_fusion
  34.6 31.5 %all_to_all.10 = bf16[8,1,16,4096]{3,2,1,0:T(8,128)(2,1)} all-to-all(bf16[8,1,16,4096]{3,2,1,0:T(8,128)(2,1)S(1)} %broadcast_select_fusion), channel_id=1, replica_groups=mesh['ep'=8,'tp'=4] {'ep'}, dimensions={0} | all-to-all | bytes 2097152 | tf_op jit(solution)/shard_map/all_to_all | solution.py:125
  67.6 31.4 %all-gather.15.cloned.1.call-done = bf16[8,1,64,4096]{3,2,0,1:T(8,128)(2,1)} async-done(((bf16[8,1,16,4096]{3,2,0,1:T(8,128)(2,1)}), bf16[8,1,64,4096]{3,2,0,1:T(8,128)(2,1)}) %all-gather.15.cloned.1.call-update) | async-done | bytes 4194320 | tf_op jit(solution)/shard_map/all_gather | solution.py:126
  98.9 5.9 %fusion.27 = f32[8,1,64,512]{3,2,0,1:T(8,128)S(1)} fusion(bf16[1,4096,512]{2,1,0:T(8,128)(2,1)} %param.25, bf16[8,1,64,4096]{3,2,0,1:T(8,128)(2,1)} %all-gather.15.cloned.1.call-done), kind=kOutput, calls=%fused_computation.33 | convolution fusion | flops 2147483648 | bytes 9437184 | tf_op jit(solution)/shard_map/sxcd,xdf->sxcf/dot_general | solution.py:127
  104.9 3.2 fusion.42
  109.6 64.3 %all-gather.7.cloned.1.call-done = bf16[4096,512]{1,0:T(8,128)(2,1)} async-done(((bf16[512,512]{1,0:T(8,128)(2,1)}), bf16[4096,512]{1,0:T(8,128)(2,1)}) %all-gather.7.cloned.1.call-update) | async-done | bytes 4194320 | tf_op jit(solution)/shard_map/all_gather | solution.py:87
  173.9 6.5 %copy.58 = bf16[8,512,512]{1,2,0:T(8,128)(2,1)} copy(bf16[8,512,512]{2,1,0:T(8,128)(2,1)} %bitcast.117) | data formatting | bytes 8388608
  180.3 66.9 %all-gather.9.cloned.1.call-done = bf16[4096,512]{1,0:T(8,128)(2,1)} async-done(((bf16[512,512]{1,0:T(8,128)(2,1)}), bf16[4096,512]{1,0:T(8,128)(2,1)}) %all-gather.9.cloned.1.call-update) | async-done | bytes 4194320 | tf_op jit(solution)/shard_map/all_gather | solution.py:88
  247.2 6.5 %copy.60 = bf16[8,512,512]{1,2,0:T(8,128)(2,1)} copy(bf16[8,512,512]{2,1,0:T(8,128)(2,1)} %bitcast.118) | data formatting | bytes 8388608
  253.8 20.4 %while.16 = (s32[]{:T(128)}, f32[4,512]{1,0:T(4,128)S(1)}, f32[4,512]{1,0:T(4,128)S(1)}, f32[4,512,128]{2,1,0:T(8,128)S(1)}, s32[8]{0:T(128)S(1)}, /*index=5*/s3...) while((s32[]{:T(128)}, f32[4,512]{1,0:T(4,128)S(1)}, ...), condition=%wide.region_5.6_spmd.clone.clone, body=%wide.region_0.5_spmd.clone.clone.sunk | while | flops 555488256 | bytes 19607904 | solution.py:96
  255.1 10.0 %conditional.4 = ((f32[4,512]{1,0:T(4,128)S(1)}, f32[4,512]{1,0:T(4,128)S(1)}, f32[4,512,128]{2,1,0:T(8,128)S(1)})) conditional(s32[]{:T(128)} %convert_element_type.100, (f32[4,512]{1,0:T(4,128)S(1)}, f32[4,512]{1,0:T(4,128)S(1)}, f32[4,512,128]{2,1,0:T(8,128)S(1)}) %tuple.54, (s32[]{:T(128)}, s32[]{:T(128)}, bf16[8,512,512]{1,2,0:T(8,128)(2,1)}, ...), branch_computations={%region_1.1_spmd, %region_2.4_spmd} | conditional | flops 555488256 | bytes 19605586 | solution.py:77
  258.7 1.3 constant_dynamic-slice_fusion
  259.9 1.4 fusion.4
  261.4 1.4 fusion.3
  262.8 2.3 fusion.8
  275.5 6.1 %fusion.24 = bf16[8,1,64,1024]{3,2,1,0:T(8,128)(2,1)} fusion(bf16[8,64,2048]{2,1,0:T(8,128)(2,1)} %bitcast.129, bf16[1,2048,1024]{2,1,0:T(8,128)(2,1)} %param.27), kind=kOutput, calls=%fused_computation.32 | convolution fusion | flops 2148007936 | bytes 7340032 | tf_op jit(solution)/shard_map/sxcf,xfd->sxcd/dot_general | solution.py:144
  281.7 72.9 %all-to-all-start.1 = ((bf16[8,1,64,1024]{3,2,1,0:T(8,128)(2,1)}), bf16[8,1,64,1024]{3,2,1,0:T(8,128)(2,1)S(1)}, u32[]{:S(2)}, u32[]{:S(2)}) async-start(bf16[8,1,64,1024]{3,2,1,0:T(8,128)(2,1)} %fusion.24), calls=%async_computation.1 | async-start | bytes 2097152 | tf_op jit(solution)/shard_map/all_to_all | solution.py:147
  355.1 11.4 %all-gather.11.cloned.1.call-done = bf16[512,2048]{0,1:T(8,128)(2,1)} async-done(((bf16[512,512]{0,1:T(8,128)(2,1)}), bf16[512,2048]{0,1:T(8,128)(2,1)}) %all-gather.11.cloned.1.call-update) | async-done | bytes 2097168 | tf_op jit(solution)/shard_map/all_gather | solution.py:138
  366.5 6.1 %convolution_convert_fusion = bf16[512,1024]{1,0:T(8,128)(2,1)} fusion(bf16[512,2048]{0,1:T(8,128)(2,1)} %all-gather.11.cloned.1.call-done, bf16[2048,1024]{1,0:T(8,128)(2,1)} %param.20), kind=kOutput, calls=%fused_computation.31 | convolution fusion | flops 2148007936 | bytes 7340032 | tf_op jit(solution)/shard_map/dot_general | solution.py:137
  372.7 7.7 %all-to-all-done.1 = bf16[8,1,64,1024]{3,2,1,0:T(8,128)(2,1)S(1)} async-done(((bf16[8,1,64,1024]{3,2,1,0:T(8,128)(2,1)}), bf16[8,1,64,1024]{3,2,1,0:T(8,128)(2,1)S(1)}, u32[]{:S(2)}, u32[]{:S(2)}) %all-to-all-start.1) | async-done | bytes 1048608 | tf_op jit(solution)/shard_map/all_to_all | solution.py:147
  381.7 2.3 multiply_reduce_fusion
  (92 shorter events, 18.4 us)
Async XLA Ops:
  7.2 23.8 %all-gather.13.cloned.1.call-start = ((), (), s32[]{:S(2)}) async-start(), calls=%async_computation.5 | async-start | bytes 1310720 | tf_op jit(solution)/shard_map/all_gather | solution.py:108
  11.3 87.6 %all-gather.15.cloned.1.call-start = ((), (), s32[]{:S(2)}) async-start(), calls=%async_computation.6 | async-start | bytes 5242880 | tf_op jit(solution)/shard_map/all_gather | solution.py:126
  66.2 107.7 %all-gather.7.cloned.1.call-start = ((), (), s32[]{:S(2)}) async-start(), calls=%async_computation.2 | async-start | bytes 4718592 | tf_op jit(solution)/shard_map/all_gather | solution.py:87
  66.9 180.3 %all-gather.9.cloned.1.call-start = ((), (), s32[]{:S(2)}) async-start(), calls=%async_computation.3 | async-start | bytes 4718592 | tf_op jit(solution)/shard_map/all_gather | solution.py:88
  67.5 208.0 %all-gather.17.cloned.1.call-start = ((), (), s32[]{:S(2)}) async-start(), calls=%async_computation.7 | async-start | bytes 2621440 | tf_op jit(solution)/shard_map/all_gather | solution.py:142
  98.9 5.9 %copy-start.3 = (bf16[1,4096,512]{2,1,0:T(8,128)(2,1)S(1)}, bf16[1,4096,512]{2,1,0:T(8,128)(2,1)}, u32[]{:S(2)}) copy-start(bf16[1,4096,512]{2,1,0:T(8,128)(2,1)} %param.26) | copy-start | bytes 12582916
  98.9 5.9 %copy-start.4 = (bf16[8,1,64,4096]{3,2,0,1:T(8,128)(2,1)S(1)}, bf16[8,1,64,4096]{3,2,0,1:T(8,128)(2,1)}, u32[]{:S(2)}) copy-start(bf16[8,1,64,4096]{3,2,0,1:T(8,128)(2,1)} %all-gather.15.cloned.1.call-done) | copy-start | bytes 12582916
  104.9 3.5 copy-start
  108.1 258.4 %all-gather.11.cloned.1.call-start = ((), (), s32[]{:S(2)}) async-start(), calls=%async_computation.4 | async-start | bytes 2621440 | tf_op jit(solution)/shard_map/all_gather | solution.py:138
  275.5 79.3 %copy-start.1 = (s32[128,2]{0,1:T(2,128)S(1)}, s32[128,2]{0,1:T(2,128)}, u32[]{:S(2)}) copy-start(s32[128,2]{0,1:T(2,128)} %param.23) | copy-start | bytes 3076
  275.5 79.5 %copy-start.2 = (f32[128,2]{0,1:T(2,128)S(1)}, f32[128,2]{0,1:T(2,128)}, u32[]{:S(2)}) copy-start(f32[128,2]{0,1:T(2,128)} %param.24) | copy-start | bytes 3076
  281.7 98.6 %all-to-all-start.1 = ((bf16[8,1,64,1024]{3,2,1,0:T(8,128)(2,1)}), bf16[8,1,64,1024]{3,2,1,0:T(8,128)(2,1)S(1)}, u32[]{:S(2)}, u32[]{:S(2)}) async-start(bf16[8,1,64,1024]{3,2,1,0:T(8,128)(2,1)} %fusion.24), calls=%async_computation.1 | async-start | bytes 2097152 | tf_op jit(solution)/shard_map/all_to_all | solution.py:147
Sparse Core Ops, SparseCore 0:
  11.5 19.4 all-gather.12
  66.3 32.5 all-gather.14
  101.1 72.7 all-gather.6
  175.9 71.3 all-gather.8
  248.6 21.0 all-gather.16
  275.6 90.8 all-gather.10
where the time goes:
time: 392 us; the launch traced here: 391 us
  waiting for transfers between devices  198 us (51%)
  starting transfers between devices  73.3 us (19%)
  blocking collectives  31.5 us (8%)
  local copies, waits for them, and re-layouts  30 us (8%)
  matrix products  25.1 us (6%)
  between operations  14.3 us (4%)
  other arithmetic  11.3 us (3%)
  loops' own time  7.47 us (2%)
    all_to_all x1, starting transfers between devices, body(): lax.all_to_all(leaving, 'ep', split_axis=0, concat_axis=0, tiled=True)  72.9 us
    all_gather x1, waiting for transfers between devices, body(): value_piece = lax.all_gather(values, 'ep', axis=0, tiled=True)  66.9 us
    all_gather x1, waiting for transfers between devices, body(): key_piece = lax.all_gather(key_rows, 'ep', axis=0, tiled=True)  64.3 us
    all_to_all x1, blocking collectives, body(): lax.all_to_all(outgoing, 'ep', split_axis=0, concat_axis=0, tiled=True)  31.5 us
    all_gather x1, waiting for transfers between devices, body(): arrived_rows = lax.all_gather(arrived, 'tp', axis=2, tiled=True)  31.4 us
    all_gather x1, waiting for transfers between devices, body(): group_rows = lax.all_gather(normed, 'tp', axis=0, tiled=True)  14.9 us
    unnamed x16, local copies, waits for them, and re-layouts  14.4 us
    all_gather x1, waiting for transfers between devices, body(): lax.all_gather(attended, 'tp', axis=1, tiled=True)  11.4 us
  transfers between devices with their start and end apart: 7, of which 6 were waited for; matrix products, arithmetic and copies ran while one was open for 14% of the time, Pallas kernels for 0%

commit v1 on v0

--- a/solution.py
+++ b/solution.py
@@ -4,6 +4,17 @@
 from jax.sharding import PartitionSpec as P
 
 EPSILON = 1e-05
+
+
+def gather_by_hops(block, mesh_axis, dim):
+    peers = lax.axis_size(mesh_axis)
+    hops = [(i, (i + 1) % peers) for i in range(peers)]
+    parts = [block]
+    for stride in range(1, peers):
+        parts = [lax.ppermute(parts[0], mesh_axis, hops), *parts]
+    full = jnp.concatenate(parts, axis=dim)
+    shift = (lax.axis_index(mesh_axis) + 1) * parts[-1].shape[dim]
+    return jnp.roll(full, shift, axis=dim)
 
 
 def slot_places(route_rows, experts, capacity):
@@ -123,7 +134,7 @@
     )
     outgoing = jnp.take(group_rows, part_table, axis=0, mode="fill", fill_value=0)
     arrived = lax.all_to_all(outgoing, "ep", split_axis=0, concat_axis=0, tiled=True)
-    arrived_rows = lax.all_gather(arrived, "tp", axis=2, tiled=True)
+    arrived_rows = gather_by_hops(arrived, "tp", 2)
     gate_part = jnp.einsum(
         "sxcd,xdf->sxcf", arrived_rows, gate_weight, preferred_element_type=jnp.float32
     )

time: 392 us -> 342 us (0.87)
  waiting for transfers between devices: 198 us -> 131 us
  blocking collectives: 31.5 us -> 48.3 us
  local copies, waits for them, and re-layouts: 30 us -> 34.3 us
    all_gather x1, waiting for transfers between devices: 64.3 us -> 0.01 us  [body(): key_piece = lax.all_gather(key_rows, 'ep', axis=0, tiled=True)]
    ppermute x0 -> x3, waiting for transfers between devices: none -> 42.7 us  [gather_by_hops(): parts = [lax.ppermute(parts[0], mesh_axis, hops), *parts]]
    all_gather x1 -> x0, waiting for transfers between devices: 31.4 us -> none  [body(): arrived_rows = lax.all_gather(arrived, 'tp', axis=2, tiled=True)]
    all_to_all x1, blocking collectives: 31.5 us -> 48.3 us  [body(): lax.all_to_all(outgoing, 'ep', split_axis=0, concat_axis=0, tiled=True)]
    all_gather x1, waiting for transfers between devices: 66.9 us -> 54 us  [body(): value_piece = lax.all_gather(values, 'ep', axis=0, tiled=True)]
    unnamed x16 -> x23, local copies, waits for them, and re-layouts: 14.4 us -> 18.3 us
  transfers between devices with their start and end apart: 7 -> 9, of which waited for: 6 -> 7; matrix products, arithmetic and copies ran while one was open for 14% -> 17% of each run, Pallas kernels for 0% -> 0%
where the time goes in v1:
time: 342 us; the launch traced here: 340 us
  waiting for transfers between devices  131 us (38%)
  starting transfers between devices  73 us (21%)
  blocking collectives  48.3 us (14%)
  local copies, waits for them, and re-layouts  34.3 us (10%)
  matrix products  21.5 us (6%)
  between operations  14 us (4%)
  other arithmetic  11.3 us (3%)
  loops' own time  7.27 us (2%)
    all_to_all x1, starting transfers between devices, body(): lax.all_to_all(leaving, 'ep', split_axis=0, concat_axis=0, tiled=True)  72.6 us
    all_gather x1, waiting for transfers between devices, body(): value_piece = lax.all_gather(values, 'ep', axis=0, tiled=True)  54 us
    all_to_all x1, blocking collectives, body(): lax.all_to_all(outgoing, 'ep', split_axis=0, concat_axis=0, tiled=True)  48.3 us
    ppermute x3, waiting for transfers between devices, gather_by_hops(): parts = [lax.ppermute(parts[0], mesh_axis, hops), *parts]  42.7 us
    unnamed x23, local copies, waits for them, and re-layouts  18.3 us
    all_gather x1, waiting for transfers between devices, body(): group_rows = lax.all_gather(normed, 'tp', axis=0, tiled=True)  14.1 us
    all_gather x1, waiting for transfers between devices, body(): lax.all_gather(attended, 'tp', axis=1, tiled=True)  11.4 us
    all_to_all x1, waiting for transfers between devices, body(): lax.all_to_all(leaving, 'ep', split_axis=0, concat_axis=0, tiled=True)  7.68 us
  transfers between devices with their start and end apart: 9, of which 7 were waited for; matrix products, arithmetic and copies ran while one was open for 17% of the time, Pallas kernels for 0%

profile of v1, /device:TPU:0, one launch (start us, length us, event | category | flops | bytes accessed | tf_op | source)
XLA Modules:
  0.0 340.5 jit_solution(4414645417046121677)
XLA Ops:
  9.5 1.8 fusion.43
  15.1 1.4 scatter_custom_fusion
  16.8 14.1 %all-gather.12.cloned.1.call-done = bf16[128,4096]{1,0:T(8,128)(2,1)} async-done(((bf16[32,4096]{1,0:T(8,128)(2,1)}), bf16[128,4096]{1,0:T(8,128)(2,1)}) %all-gather.12.cloned.1.call-update) | async-done | bytes 1048592 | tf_op jit(solution)/shard_map/all_gather | solution.py:119
  30.9 3.6 %gather_fusion = bf16[128,4096]{1,0:T(8,128)(2,1)S(1)} fusion(bf16[128,4096]{1,0:T(8,128)(2,1)} %all-gather.12.cloned.1.call-done, s32[1024]{0:T(1024)S(1)} %pad_clamp_fusion.1), kind=kCustom, calls=%fused_computation | custom fusion | bytes 2097664 | tf_op jit(solution)/shard_map/jit(_take)/gather | solution.py:135
  34.6 48.3 %all_to_all.10 = bf16[8,1,16,4096]{3,2,1,0:T(8,128)(2,1)S(1)} all-to-all(bf16[8,1,16,4096]{3,2,1,0:T(8,128)(2,1)S(1)} %broadcast_select_fusion), channel_id=1, replica_groups=mesh['ep'=8,'tp'=4] {'ep'}, dimensions={0} | all-to-all | bytes 2097152 | tf_op jit(solution)/shard_map/all_to_all | solution.py:136
  83.0 14.1 %collective-permute-done = bf16[8,1,16,4096]{3,2,1,0:T(8,128)(2,1)S(1)} collective-permute-done((bf16[8,1,16,4096]{3,2,1,0:T(8,128)(2,1)S(1)}, bf16[8,1,16,4096]{3,2,1,0:T(8,128)(2,1)S(1)}, u32[]{:S(2)}, u32[]{:S(2)}) %collective-permute-start) | collective-permute-done | bytes 1048608 | tf_op jit(solution)/shard_map/ppermute | solution.py:14
  97.1 14.2 %collective-permute-done.1 = bf16[8,1,16,4096]{3,2,1,0:T(8,128)(2,1)S(1)} collective-permute-done((bf16[8,1,16,4096]{3,2,1,0:T(8,128)(2,1)S(1)}, bf16[8,1,16,4096]{3,2,1,0:T(8,128)(2,1)S(1)}, u32[]{:S(2)}, u32[]{:S(2)}) %collective-permute-start.1) | collective-permute-done | bytes 1048608 | tf_op jit(solution)/shard_map/ppermute | solution.py:14
  111.4 14.3 %collective-permute-done.2 = bf16[8,1,16,4096]{3,2,1,0:T(8,128)(2,1)} collective-permute-done((bf16[8,1,16,4096]{3,2,1,0:T(8,128)(2,1)S(1)}, bf16[8,1,16,4096]{3,2,1,0:T(8,128)(2,1)}, u32[]{:S(2)}, u32[]{:S(2)}) %collective-permute-start.2) | collective-permute-done | bytes 1048608 | tf_op jit(solution)/shard_map/ppermute | solution.py:14
  127.3 1.4 constant_dynamic-update-slice_fusion.3
  129.8 2.3 fusion.29
  132.1 3.2 multiply_convert_fusion
  136.8 6.5 %copy.57 = bf16[8,512,512]{1,2,0:T(8,128)(2,1)} copy(bf16[8,512,512]{2,1,0:T(8,128)(2,1)} %bitcast.110) | data formatting | bytes 8388608
  143.3 54.0 %all-gather.8.cloned.1.call-done = bf16[4096,512]{1,0:T(8,128)(2,1)} async-done(((bf16[512,512]{1,0:T(8,128)(2,1)}), bf16[4096,512]{1,0:T(8,128)(2,1)}) %all-gather.8.cloned.1.call-update) | async-done | bytes 4194320 | tf_op jit(solution)/shard_map/all_gather | solution.py:99
  197.3 6.5 %copy.59 = bf16[8,512,512]{1,2,0:T(8,128)(2,1)} copy(bf16[8,512,512]{2,1,0:T(8,128)(2,1)} %bitcast.111) | data formatting | bytes 8388608
  203.9 20.4 %while.16 = (s32[]{:T(128)}, f32[4,512]{1,0:T(4,128)S(1)}, f32[4,512]{1,0:T(4,128)S(1)}, f32[4,512,128]{2,1,0:T(8,128)S(1)}, s32[8]{0:T(128)S(1)}, /*index=5*/s3...) while((s32[]{:T(128)}, f32[4,512]{1,0:T(4,128)S(1)}, ...), condition=%wide.region_5.6_spmd.clone.clone, body=%wide.region_0.5_spmd.clone.clone.sunk | while | flops 555488256 | bytes 19607896 | solution.py:107
  205.2 9.9 %conditional.4 = ((f32[4,512]{1,0:T(4,128)S(1)}, f32[4,512]{1,0:T(4,128)S(1)}, f32[4,512,128]{2,1,0:T(8,128)S(1)})) conditional(s32[]{:T(128)} %convert_element_type.100, (f32[4,512]{1,0:T(4,128)S(1)}, f32[4,512]{1,0:T(4,128)S(1)}, f32[4,512,128]{2,1,0:T(8,128)S(1)}) %tuple.54, (s32[]{:T(128)}, s32[]{:T(128)}, bf16[8,512,512]{1,2,0:T(8,128)(2,1)}, ...), branch_computations={%region_1.1_spmd, %region_2.4_spmd} | conditional | flops 555488256 | bytes 19605586 | solution.py:88
  210.0 1.4 fusion.4
  212.8 2.3 fusion.8
  225.7 6.1 %fusion.26 = bf16[8,1,64,1024]{3,2,1,0:T(8,128)(2,1)} fusion(bf16[8,64,2048]{2,1,0:T(8,128)(2,1)} %bitcast.121, bf16[1,2048,1024]{2,1,0:T(8,128)(2,1)} %param.27), kind=kOutput, calls=%fused_computation.34 | convolution fusion | flops 2148007936 | bytes 7340032 | tf_op jit(solution)/shard_map/sxcf,xfd->sxcd/dot_general | solution.py:155
  231.9 72.6 %all-to-all-start.1 = ((bf16[8,1,64,1024]{3,2,1,0:T(8,128)(2,1)}), bf16[8,1,64,1024]{3,2,1,0:T(8,128)(2,1)S(1)}, u32[]{:S(2)}, u32[]{:S(2)}) async-start(bf16[8,1,64,1024]{3,2,1,0:T(8,128)(2,1)} %fusion.26), calls=%async_computation.1 | async-start | bytes 2097152 | tf_op jit(solution)/shard_map/all_to_all | solution.py:158
  305.0 11.4 %all-gather.10.cloned.1.call-done = bf16[512,2048]{0,1:T(8,128)(2,1)} async-done(((bf16[512,512]{0,1:T(8,128)(2,1)}), bf16[512,2048]{0,1:T(8,128)(2,1)}) %all-gather.10.cloned.1.call-update) | async-done | bytes 2097168 | tf_op jit(solution)/shard_map/all_gather | solution.py:149
  316.4 6.1 %convolution_convert_fusion = bf16[512,1024]{1,0:T(8,128)(2,1)} fusion(bf16[512,2048]{0,1:T(8,128)(2,1)} %all-gather.10.cloned.1.call-done, bf16[2048,1024]{1,0:T(8,128)(2,1)} %param.20), kind=kOutput, calls=%fused_computation.33 | convolution fusion | flops 2148007936 | bytes 7340032 | tf_op jit(solution)/shard_map/dot_general | solution.py:148
  322.5 7.7 %all-to-all-done.1 = bf16[8,1,64,1024]{3,2,1,0:T(8,128)(2,1)S(1)} async-done(((bf16[8,1,64,1024]{3,2,1,0:T(8,128)(2,1)}), bf16[8,1,64,1024]{3,2,1,0:T(8,128)(2,1)S(1)}, u32[]{:S(2)}, u32[]{:S(2)}) %all-to-all-start.1) | async-done | bytes 1048608 | tf_op jit(solution)/shard_map/all_to_all | solution.py:158
  331.6 2.3 multiply_reduce_fusion
  (103 shorter events, 23.3 us)
Async XLA Ops:
  7.2 23.8 %all-gather.12.cloned.1.call-start = ((), (), s32[]{:S(2)}) async-start(), calls=%async_computation.5 | async-start | bytes 1310720 | tf_op jit(solution)/shard_map/all_gather | solution.py:119
  11.3 125.5 %all-gather.6.cloned.1.call-start = ((), (), s32[]{:S(2)}) async-start(), calls=%async_computation.2 | async-start | bytes 4718592 | tf_op jit(solution)/shard_map/all_gather | solution.py:98
  12.1 185.2 %all-gather.8.cloned.1.call-start = ((), (), s32[]{:S(2)}) async-start(), calls=%async_computation.3 | async-start | bytes 4718592 | tf_op jit(solution)/shard_map/all_gather | solution.py:99
  82.9 14.2 %collective-permute-start = (bf16[8,1,16,4096]{3,2,1,0:T(8,128)(2,1)S(1)}, bf16[8,1,16,4096]{3,2,1,0:T(8,128)(2,1)S(1)}, u32[]{:S(2)}, u32[]{:S(2)}) collective-permute-start(bf16[8,1,16,4096]{3,2,1,0:T(8,128)(2,1)S(1)} %all_to_all.10), channel_id=1, source_target_pairs={{0,1},{1,2},{2,3},{3,0},{4,5},{5,6},{6,7},{7,4},{8,9},{9,10},{10,1... | collective-permute-start | bytes 3145736 | tf_op jit(solution)/shard_map/ppermute | solution.py:14
  82.9 142.7 %all-gather.14.cloned.1.call-start = ((), (), s32[]{:S(2)}) async-start(), calls=%async_computation.6 | async-start | bytes 2621440 | tf_op jit(solution)/shard_map/all_gather | solution.py:153
  97.1 14.2 %collective-permute-start.1 = (bf16[8,1,16,4096]{3,2,1,0:T(8,128)(2,1)S(1)}, bf16[8,1,16,4096]{3,2,1,0:T(8,128)(2,1)S(1)}, u32[]{:S(2)}, u32[]{:S(2)}) collective-permute-start(bf16[8,1,16,4096]{3,2,1,0:T(8,128)(2,1)S(1)} %collective-permute-done), channel_id=1, source_target_pairs={{0,1},{1,2},{2,3},{3,0},{4,5},{5,6},{6,7},{7,4},{8,9},{9,10},{10,1... | collective-permute-start | bytes 3145736 | tf_op jit(solution)/shard_map/ppermute | solution.py:14
  111.4 14.3 %collective-permute-start.2 = (bf16[8,1,16,4096]{3,2,1,0:T(8,128)(2,1)S(1)}, bf16[8,1,16,4096]{3,2,1,0:T(8,128)(2,1)}, u32[]{:S(2)}, u32[]{:S(2)}) collective-permute-start(bf16[8,1,16,4096]{3,2,1,0:T(8,128)(2,1)S(1)} %collective-permute-done.1), channel_id=1, source_target_pairs={{0,1},{1,2},{2,3},{3,0},{4,5},{5,6},{6,7},{7,4},{8,9},{9,10},{10,1... | collective-permute-start | bytes 3145736 | tf_op jit(solution)/shard_map/ppermute | solution.py:14
  127.3 2.5 copy-start.3
  129.8 2.3 copy-start.4
  132.1 3.5 %copy-start = (bf16[512,512]{1,0:T(8,128)(2,1)S(1)}, bf16[512,512]{1,0:T(8,128)(2,1)}, u32[]{:S(2)}) copy-start(bf16[512,512]{1,0:T(8,128)(2,1)} %param.16) | copy-start | bytes 1572868
  135.4 181.0 %all-gather.10.cloned.1.call-start = ((), (), s32[]{:S(2)}) async-start(), calls=%async_computation.4 | async-start | bytes 2621440 | tf_op jit(solution)/shard_map/all_gather | solution.py:149
  225.7 79.0 %copy-start.1 = (s32[128,2]{0,1:T(2,128)S(1)}, s32[128,2]{0,1:T(2,128)}, u32[]{:S(2)}) copy-start(s32[128,2]{0,1:T(2,128)} %param.23) | copy-start | bytes 3076
  225.7 79.2 %copy-start.2 = (f32[128,2]{0,1:T(2,128)S(1)}, f32[128,2]{0,1:T(2,128)}, u32[]{:S(2)}) copy-start(f32[128,2]{0,1:T(2,128)} %param.24) | copy-start | bytes 3076
  231.9 98.4 %all-to-all-start.1 = ((bf16[8,1,64,1024]{3,2,1,0:T(8,128)(2,1)}), bf16[8,1,64,1024]{3,2,1,0:T(8,128)(2,1)S(1)}, u32[]{:S(2)}, u32[]{:S(2)}) async-start(bf16[8,1,64,1024]{3,2,1,0:T(8,128)(2,1)} %fusion.26), calls=%async_computation.1 | async-start | bytes 2097152 | tf_op jit(solution)/shard_map/all_to_all | solution.py:158
Sparse Core Ops, SparseCore 0:
  11.5 19.4 all-gather.11
  33.1 90.7 all-gather.5
  125.9 71.3 all-gather.7
  198.7 21.0 all-gather.13
  225.8 90.5 all-gather.9
